TPU v7x, 32 devices: a whole 2x2x4 slice. The times are simulated.
32 devices in a mesh: sp: 8 (over z, x), tp: 4 (over y, core).
Axes of the slice: x: 2, y: 2, z: 4, core: 2. Of those that a mesh axis runs over, the one named last changes fastest.
Arguments:
- tokens: bfloat16 [2048, 1024], P(('sp', 'tp')), may hold values from -6 to 6
- norm_gain: float32 [1024], replicated, may hold values from 0.1 to 1.9
- w_query: bfloat16 [1024, 1024], P('sp', 'tp'), may hold values from -0.1875 to 0.1875
- w_key: bfloat16 [1024, 1024], P('sp', 'tp'), may hold values from -0.1875 to 0.1875
- w_value: bfloat16 [1024, 1024], P('sp', 'tp'), may hold values from -0.1875 to 0.1875
- w_forget: bfloat16 [1024, 16], P('sp', 'tp'), may hold values from -0.375 to 0.375
- forget_offset: float32 [16], P('tp'), may hold values from 1 to 3.5
- w_out_t: bfloat16 [1024, 1024], P('sp', 'tp'), may hold values from -0.1875 to 0.1875
- out_gain: float32 [1024], replicated, may hold values from 0.1 to 1.9
Outputs:
- mixed: bfloat16 [2048, 1024], P(('sp', 'tp'))
All inputs are finite; a program needn't handle non-finite values.
Results may differ from a plain program's by a relative error of at most 0.015.
Values may be sent and summed in bfloat16 or wider, within the bound.
A program may use at most 192 MiB of HBM per device.

v0:
```python
import jax
import jax.numpy as jnp
from jax import lax
from jax.sharding import PartitionSpec as P

HEAD_DIM = 64


norm_eps = 1e-06
masked_score = -1e30


def on_whole(shard, axis, dim, work):
    return work(lax.all_gather(shard, axis, axis=dim, tiled=True), jnp.int32(0))


def over_all(section, axis, dim, turn, start):
    def gathered(part):
        return lax.all_gather(part, axis, axis=dim, tiled=True)

    return turn(start, jax.tree.map(gathered, section), jnp.int32(0))


def own_rows(portion, width, axis):
    count = width * lax.axis_size(axis)
    sent = portion(jnp.int32(0), count).astype(jnp.bfloat16)
    return lax.psum_scatter(sent, axis, scatter_dimension=0, tiled=True).astype(jnp.float32)


def rms_norm(values_in, gain_row):
    floats = values_in.astype(jnp.float32)
    scale_row = lax.rsqrt(jnp.mean(floats * floats, axis=-1, keepdims=True) + norm_eps)
    return (floats * scale_row * gain_row).astype(jnp.bfloat16)


def on_device(
    tokens, norm_gain, w_query, w_key, w_value, w_forget, forget_offset, w_out_t, out_gain
):
    normed = rms_norm(tokens, norm_gain)
    width_local = w_query.shape[1]
    heads_local = w_forget.shape[1]
    tok_block = normed.shape[0] * lax.axis_size("tp")
    total_tokens = tok_block * lax.axis_size("sp")
    full_query, full_key, full_value, full_forget, out_weight = (
        lax.all_gather(w_query, "sp", axis=0, tiled=True),
        lax.all_gather(w_key, "sp", axis=0, tiled=True),
        lax.all_gather(w_value, "sp", axis=0, tiled=True),
        lax.all_gather(w_forget, "sp", axis=0, tiled=True),
        lax.all_gather(w_out_t, "sp", axis=0, tiled=True),
    )
    joined = jnp.concatenate([full_query, full_key, full_value, full_forget], axis=1)

    def project(row_piece, first_row):
        return jnp.dot(row_piece, joined, preferred_element_type=jnp.float32)

    projected_cols = on_whole(normed, "tp", 0, project)
    head_shape = (tok_block, heads_local, HEAD_DIM)
    queries = projected_cols[:, :width_local].astype(jnp.bfloat16).reshape(head_shape)
    keys_here = (
        projected_cols[:, width_local : 2 * width_local].astype(jnp.bfloat16).reshape(head_shape)
    )
    values_here = (
        projected_cols[:, 2 * width_local : 3 * width_local]
        .astype(jnp.bfloat16)
        .reshape(head_shape)
    )
    logits = (
        projected_cols[:, 3 * width_local :] + forget_offset + jnp.log(jnp.float32(total_tokens))
    )
    log_gates = jax.nn.log_sigmoid(logits)
    all_gates = lax.all_gather(log_gates, "sp", axis=0, tiled=True)
    cumulative = jnp.cumsum(all_gates, axis=0)
    offset = lax.axis_index("sp") * tok_block
    cum_query = lax.dynamic_slice_in_dim(cumulative, offset, tok_block, 0)
    query_pos = offset + jnp.arange(tok_block, dtype=jnp.int32)
    score_scale = HEAD_DIM ** (-0.5)

    def absorb(state_now, pieces, first_row):
        run_max, run_sum, run_acc = state_now
        key_piece, value_piece = pieces
        span_len = key_piece.shape[0]
        cum_key = lax.dynamic_slice_in_dim(cumulative, first_row, span_len, 0)
        scores = (
            jnp.einsum("qhd,khd->hqk", queries, key_piece, preferred_element_type=jnp.float32)
            * score_scale
        )
        scores = scores + cum_query.T[:, :, None] - cum_key.T[:, None, :]
        key_pos = first_row + jnp.arange(span_len, dtype=jnp.int32)
        allowed = (key_pos[None, :] <= query_pos[:, None])[None]
        scores = jnp.where(allowed, scores, masked_score)
        new_max = jnp.maximum(run_max, jnp.max(scores, axis=-1))
        shares = jnp.where(allowed, jnp.exp(scores - new_max[..., None]), 0.0)
        rescale = jnp.exp(run_max - new_max)
        new_sum = run_sum * rescale + jnp.sum(shares, axis=-1)
        new_acc = run_acc * rescale[..., None] + jnp.einsum(
            "hqk,khd->hqd", shares, value_piece.astype(jnp.float32), precision=lax.Precision.HIGHEST
        )
        return (new_max, new_sum, new_acc)

    start_state = (
        jnp.full((heads_local, tok_block), masked_score, jnp.float32),
        jnp.zeros((heads_local, tok_block), jnp.float32),
        jnp.zeros((heads_local, tok_block, HEAD_DIM), jnp.float32),
    )
    run_max, run_sum, run_acc = over_all((keys_here, values_here), "sp", 0, absorb, start_state)
    attended = (
        (run_acc / run_sum[..., None])
        .transpose(1, 0, 2)
        .reshape(tok_block, width_local)
        .astype(jnp.bfloat16)
    )
    rows_mine = tokens.shape[0]

    def out_term(first_row, row_count):
        block_rows = lax.dynamic_slice_in_dim(attended, first_row, row_count, 0)
        return lax.dot_general(
            block_rows, out_weight, (((1,), (1,)), ((), ())), preferred_element_type=jnp.float32
        )

    projected = own_rows(out_term, rows_mine, "tp")
    return rms_norm(projected, out_gain)


def solution(mesh):
    return jax.shard_map(
        on_device,
        mesh=mesh,
        in_specs=(
            P(("sp", "tp"), None),
            P(),
            P("sp", "tp"),
            P("sp", "tp"),
            P("sp", "tp"),
            P("sp", "tp"),
            P("tp"),
            P("sp", "tp"),
            P(),
        ),
        out_specs=P(("sp", "tp"), None),
        check_vma=False,
    )
```

profile of v0, /device:TPU:1, one launch (start us, length us, event | category | flops | bytes accessed | tf_op | source)
XLA Modules:
  0.0 255.4 jit_solution(14113764363407624056)
XLA Ops:
  6.5 1.1 fusion.22
  7.6 1.0 fusion.24
  8.6 8.5 %all_gather.27 = bf16[256,1024]{1,0:T(8,128)(2,1)S(1)} all-gather(bf16[64,1024]{1,0:T(8,128)(2,1)S(1)} %fusion.24), channel_id=1, replica_groups=mesh['sp'=8,'tp'=4] {'tp'}, dimensions={0}, use_global_device_ids=true | all-gather | bytes 655360 | tf_op jit(solution)/shard_map/all_gather | solution.py:14
  17.2 25.8 %all_gather.28 = bf16[1024,256]{1,0:T(8,128)(2,1)S(1)} all-gather(bf16[128,256]{1,0:T(8,128)(2,1)} %param.11), channel_id=1, replica_groups=mesh['sp'=8,'tp'=4] {'sp'}, dimensions={0}, use_global_device_ids=true | all-gather | bytes 589824 | tf_op jit(solution)/shard_map/all_gather | solution.py:45
  43.0 25.6 %all_gather.29 = bf16[1024,256]{1,0:T(8,128)(2,1)S(1)} all-gather(bf16[128,256]{1,0:T(8,128)(2,1)} %param.12), channel_id=1, replica_groups=mesh['sp'=8,'tp'=4] {'sp'}, dimensions={0}, use_global_device_ids=true | all-gather | bytes 589824 | tf_op jit(solution)/shard_map/all_gather | solution.py:46
  68.5 25.7 %all_gather.30 = bf16[1024,256]{1,0:T(8,128)(2,1)S(1)} all-gather(bf16[128,256]{1,0:T(8,128)(2,1)} %param.13), channel_id=1, replica_groups=mesh['sp'=8,'tp'=4] {'sp'}, dimensions={0}, use_global_device_ids=true | all-gather | bytes 589824 | tf_op jit(solution)/shard_map/all_gather | solution.py:47
  94.2 17.0 %all_gather.31 = bf16[1024,4]{0,1:T(4,128)(2,1)S(1)} all-gather(bf16[128,4]{0,1:T(4,128)(2,1)} %param.14), channel_id=1, replica_groups=mesh['sp'=8,'tp'=4] {'sp'}, dimensions={0}, use_global_device_ids=true | all-gather | bytes 9216 | tf_op jit(solution)/shard_map/all_gather | solution.py:48
  111.2 0.2 copy.11
  111.4 0.8 fusion.36
  112.2 0.7 fusion.35
  112.9 0.0 all-gather.3.cloned.1.call-update
  113.0 0.0 all-gather.5.cloned.1.call-start
  113.0 0.7 all-gather.5.cloned.1.call-update
  113.7 0.0 reduce-scatter.2.cloned.1.call-start
  113.8 0.1 fusion.28
  113.9 24.1 %all_gather.33 = f32[2048,4]{0,1:T(4,128)S(1)} all-gather(f32[256,4]{0,1:T(4,128)S(1)} %fusion.28), channel_id=1, replica_groups=mesh['sp'=8,'tp'=4] {'sp'}, dimensions={0}, use_global_device_ids=true | all-gather | bytes 36864 | tf_op jit(solution)/shard_map/all_gather | solution.py:71
  138.0 1.1 reduce-window.6
  139.1 0.2 slice_reduce_fusion
  139.3 0.2 reduce-window.9
  139.4 0.1 add_bitcast_fusion
  139.6 0.4 iota_compare_fusion
  139.9 25.7 %all_gather.35 = bf16[1024,256]{1,0:T(8,128)(2,1)S(1)} all-gather(bf16[128,256]{1,0:T(8,128)(2,1)S(1)} %copy-done.1), channel_id=1, replica_groups=mesh['sp'=8,'tp'=4] {'sp'}, dimensions={0}, use_global_device_ids=true | all-gather | bytes 589824 | tf_op jit(solution)/shard_map/all_gather | solution.py:49
  165.7 3.9 %all-gather.3.cloned.1.call-done = bf16[2048,4,64]{0,2,1:T(8,128)(2,1)} async-done(((bf16[256,4,64]{0,2,1:T(8,128)(2,1)}), bf16[2048,4,64]{0,2,1:T(8,128)(2,1)}) %all-gather.3.cloned.1.call-update) | async-done | bytes 1048592 | tf_op jit(solution)/shard_map/all_gather | solution.py:19
  169.6 3.8 %fusion.2 = (f32[4,256]{1,0:T(4,128)S(1)}, f32[4,256,2048]{2,1,0:T(8,128)S(1)}) fusion(f32[4,2048]{1,0:T(4,128)S(1)} %bitcast.38, f32[4,256]{1,0:T(4,128)S(1)} %constant_dynamic-slice_fusion, pred[256,2048]{1,0:T(8,128)(4,1)S(1)} %iota_compare_fusion, bf16[256,4,64]{0,2,1:T(8,128)(2,1)S(1)} %bitcast.44, bf16[2048,4,64]{0,2,1:T(8,128)(2,1)} %all-gather.3.cloned.1.call-done), kind=kOutput, calls=%fused_computation.4 | convolution fusion | flops 278920192 | bytes 10133504 | tf_op jit(solution)/shard_map/qhd,khd->hqk/dot_general | solution.py:84
  173.4 3.2 %copy-done = f32[4,256,2048]{2,1,0:T(8,128)} copy-done((f32[4,256,2048]{2,1,0:T(8,128)}, f32[4,256,2048]{2,1,0:T(8,128)S(1)}, u32[]{:S(2)}) %copy-start) | copy-done | bytes 8388632
  176.6 3.2 %fusion = f32[4,256]{1,0:T(4,128)S(1)} fusion(f32[4,256,2048]{2,1,0:T(8,128)S(1)} %get-tuple-element.13, f32[4,256]{1,0:T(4,128)S(1)} %get-tuple-element.9, f32[4,2048]{1,0:T(4,128)S(1)} %bitcast.39, f32[4,256]{1,0:T(4,128)S(1)} %constant_dynamic-slice_fusion, pred[256,2048]{1,0:T(8,128)(4,1)S(1)} %iota_compare_fusion), kind=kLoop, calls=%fused_computation.2 | loop fusion | flops 14679040 | bytes 8957952 | tf_op jit(solution)/shard_map/reduce_sum | solution.py:94
  179.8 32.2 %all-gather.5.cloned.1.call-done = bf16[2048,4,64]{0,2,1:T(8,128)(2,1)} async-done(((bf16[256,4,64]{0,2,1:T(8,128)(2,1)}), bf16[2048,4,64]{0,2,1:T(8,128)(2,1)}) %all-gather.5.cloned.1.call-update) | async-done | bytes 1048592 | tf_op jit(solution)/shard_map/all_gather | solution.py:19
  212.1 10.4 %fusion.21 = bf16[256,4,64]{0,2,1:T(8,128)(2,1)S(1)} fusion(bf16[2048,4,64]{0,2,1:T(8,128)(2,1)} %all-gather.5.cloned.1.call-done, f32[4,256,2048]{2,1,0:T(8,128)} %copy-done, f32[4,256]{1,0:T(4,128)S(1)} %get-tuple-element.9, f32[4,2048]{1,0:T(4,128)S(1)} %bitcast.40, f32[4,256]{1,0:T(4,128)S(1)} %constant_dynamic-slice_fusion, ...), kind=kOutput, calls=%fused_computation.25 | convolution fusion | flops 1623392256 | bytes 10141696 | tf_op jit(solution)/shard_map/hqk,khd->hqd/dot_general | solution.py:95
  222.5 1.2 convolution_convert_fusion
  223.7 22.5 %reduce-scatter.2.cloned.1.call-done = bf16[64,1024]{1,0:T(8,128)(2,1)} async-done(((bf16[256,1024]{1,0:T(8,128)(2,1)}), bf16[64,1024]{1,0:T(8,128)(2,1)}) %reduce-scatter.2.cloned.1.call-update) | async-done | bytes 131088 | tf_op jit(solution)/shard_map/reduce_scatter | solution.py:27
  246.1 1.0 fusion.25
  247.2 1.7 fusion.27
  (17 shorter events, 0.1 us)
Async XLA Ops:
  6.5 107.2 %copy-start.3 = (f32[4]{0:T(128)S(1)}, f32[4]{0:T(128)}, u32[]{:S(2)}) copy-start(f32[4]{0:T(128)} %param.15) | copy-start | bytes 52
  6.5 133.4 %copy-start.1 = (bf16[128,256]{1,0:T(8,128)(2,1)S(1)}, bf16[128,256]{1,0:T(8,128)(2,1)}, u32[]{:S(2)}) copy-start(bf16[128,256]{1,0:T(8,128)(2,1)} %param.16) | copy-start | bytes 196612
  6.5 163.0 %all-gather.3.cloned.1.call-start = ((), (), s32[]{:S(2)}) async-start(), calls=%async_computation.1 | async-start | bytes 1179648 | tf_op jit(solution)/shard_map/all_gather | solution.py:19
  113.0 99.1 %all-gather.5.cloned.1.call-start = ((), (), s32[]{:S(2)}) async-start(), calls=%async_computation.2 | async-start | bytes 1179648 | tf_op jit(solution)/shard_map/all_gather | solution.py:19
  113.7 132.4 %reduce-scatter.2.cloned.1.call-start = ((), (), s32[]{:S(2)}) async-start(), calls=%async_computation.3 | async-start | bytes 655360 | tf_op jit(solution)/shard_map/reduce_scatter | solution.py:27
  173.4 3.2 %copy-start = (f32[4,256,2048]{2,1,0:T(8,128)}, f32[4,256,2048]{2,1,0:T(8,128)S(1)}, u32[]{:S(2)}) copy-start(f32[4,256,2048]{2,1,0:T(8,128)S(1)} %get-tuple-element.13) | copy-start | bytes 25165828
  212.1 35.1 %copy-start.2 = (f32[1024]{0:T(1024)S(1)}, f32[1024]{0:T(1024)}, u32[]{:S(2)}) copy-start(f32[1024]{0:T(1024)} %param.17) | copy-start | bytes 12292
Sparse Core Ops, SparseCore 0:
  113.1 56.4 all-gather.2
  171.6 40.4 all-gather.4
  223.8 22.3 reduce-scatter.1
where the time goes:
time: 257 us; the launch traced here: 255 us
  blocking collectives  152 us (59%)
  waiting for transfers between devices  59.3 us (23%)
  matrix products  16.2 us (6%)
  between operations  13.2 us (5%)
  other arithmetic  9.86 us (4%)
  local copies, waits for them, and re-layouts  4.32 us (2%)
    all_gather x2, waiting for transfers between devices, gathered(): return lax.all_gather(part, axis, axis=dim, tiled=True)  36.1 us
    all_gather x1, blocking collectives, on_device(): lax.all_gather(w_query, 'sp', axis=0, tiled=True)  25.8 us
    all_gather x1, blocking collectives, on_device(): lax.all_gather(w_out_t, 'sp', axis=0, tiled=True)  25.7 us
    all_gather x1, blocking collectives, on_device(): lax.all_gather(w_value, 'sp', axis=0, tiled=True)  25.7 us
    all_gather x1, blocking collectives, on_device(): lax.all_gather(w_key, 'sp', axis=0, tiled=True)  25.6 us
    all_gather x1, blocking collectives, on_device(): all_gates = lax.all_gather(log_gates, 'sp', axis=0, tiled=True)  24.1 us
    reduce_scatter x1, waiting for transfers between devices, own_rows(): lax.psum_scatter(sent, axis, scatter_dimension=0, tiled=True)  22.5 us
    all_gather x1, blocking collectives, on_device(): lax.all_gather(w_forget, 'sp', axis=0, tiled=True)  17 us
  transfers between devices with their start and end apart: 3, of which 3 were waited for; matrix products, arithmetic and copies ran while one was open for 4% of the time, Pallas kernels for 0%

commit v1 on v0

v1 whole, which is shorter than its diff:
```python
import functools

import jax
import jax.numpy as jnp
from jax import lax
from jax.experimental import pallas as pl
from jax.experimental.pallas import tpu as pltpu
from jax.sharding import PartitionSpec as P

HEAD_DIM = 64
LANES = 128
NORM_EPS = 1e-06
MESH = pl.DeviceIdType.MESH
F32 = jnp.float32
BF16 = jnp.bfloat16
CONTRACT_LAST = (((1,), (1,)), ((), ()))


def rms_norm(floats, gain_row):
    scale_col = lax.rsqrt(jnp.mean(floats * floats, axis=-1, keepdims=True) + NORM_EPS)
    return (floats * scale_col * gain_row).astype(BF16)


def layer_kernel(
    n_sp, n_tp, heads,
    tokens_ref, gain_ref, wq_ref, wk_ref, wv_ref, wf_ref, offset_ref, wo_ref, out_gain_ref,
    out_ref,
    normed, w_all, wo_all, kv_all, gates, q_heads, cum_query, run_max, run_acc, partial, shares,
    local_sem, send_sem, recv_sem, gate_send, gate_recv, tok_send, tok_recv, sum_send, sum_recv,
):
    sp, tp = lax.axis_index("sp"), lax.axis_index("tp")
    rows = tokens_ref.shape[0]
    w_rows, width = wq_ref.shape
    block = rows * n_tp
    half = n_sp // 2

    odd = lax.rem(sp, 2)
    place = (1 - odd) * lax.div(sp, 2) + odd * (n_sp - lax.div(sp + 1, 2))

    def index_at(position):
        position = lax.rem(position + n_sp, n_sp)
        upper = lax.div(position, half)
        return (1 - upper) * 2 * position + upper * (2 * (n_sp - position) - 1)

    right, left = index_at(place + 1), index_at(place - 1)

    def shard_w(index):
        return w_all.at[pl.ds(pl.multiple_of(index * w_rows, w_rows), w_rows), :]

    def shard_wo(index):
        return wo_all.at[pl.ds(pl.multiple_of(index * w_rows, w_rows), w_rows), :]

    def shard_kv(index):
        return kv_all.at[pl.ds(pl.multiple_of(index * block, block), block), :]

    def hop(ring, shard, way, step, index):
        return pltpu.make_async_remote_copy(
            src_ref=shard(index),
            dst_ref=shard(index),
            send_sem=send_sem.at[ring, way, step],
            recv_sem=recv_sem.at[ring, way, step],
            device_id=((right, left)[way], tp),
            device_id_type=MESH,
        )

    def ring_start(ring, shard):
        hop(ring, shard, 0, 1, sp).start()
        if half > 1:
            hop(ring, shard, 1, 1, sp).start()

    def ring_step(ring, shard, step):
        first, second = index_at(place - step), index_at(place + step)
        hop(ring, shard, 0, step, first).wait_recv()

        @pl.when(step < half)
        def _():
            hop(ring, shard, 0, step + 1, first).start()
            hop(ring, shard, 1, step, second).wait_recv()

        @pl.when(step < half - 1)
        def _():
            hop(ring, shard, 1, step + 1, second).start()

        return first, second

    def ring_drain(ring, shard):
        @pl.loop(1, half + 1)
        def _(step):
            hop(ring, shard, 0, step, sp).wait_send()

            @pl.when(step < half)
            def _():
                hop(ring, shard, 1, step, sp).wait_send()

    own_rows = pl.ds(pl.multiple_of(sp * w_rows, w_rows), w_rows)
    local = [
        pltpu.make_async_copy(ref, w_all.at[own_rows, pl.ds(i * width, width)], local_sem.at[i])
        for i, ref in enumerate((wq_ref, wk_ref, wv_ref))
    ]
    local.append(pltpu.make_async_copy(wo_ref, wo_all.at[own_rows, :], local_sem.at[3]))
    for copy in local:
        copy.start()

    barrier = pltpu.get_barrier_semaphore()
    for shift in range(1, n_sp):
        pl.semaphore_signal(
            barrier, inc=1, device_id=(lax.rem(sp + shift, n_sp), tp), device_id_type=MESH
        )
    for shift in range(1, n_tp):
        pl.semaphore_signal(
            barrier, inc=1, device_id=(sp, lax.rem(tp + shift, n_tp)), device_id_type=MESH
        )

    forget = jnp.concatenate(
        [wf_ref[...].astype(F32), jnp.zeros((w_rows, LANES - heads), F32)], axis=1
    )
    w_all[own_rows, 3 * width :] = forget.astype(BF16)
    my_rows = pl.ds(pl.multiple_of(tp * rows, rows), rows)
    normed[my_rows, :] = rms_norm(tokens_ref[...].astype(F32), gain_ref[...])
    for copy in local:
        copy.wait()
    pl.semaphore_wait(barrier, n_sp + n_tp - 2)

    ring_start(0, shard_w)

    def tok_copy(shift):
        return pltpu.make_async_remote_copy(
            src_ref=normed.at[my_rows, :],
            dst_ref=normed.at[my_rows, :],
            send_sem=tok_send.at[shift - 1],
            recv_sem=tok_recv.at[shift - 1],
            device_id=(sp, lax.rem(tp + shift, n_tp)),
            device_id_type=MESH,
        )

    for shift in range(1, n_tp):
        tok_copy(shift).start()

    @pl.loop(1, half + 1)
    def _(step):
        ring_step(0, shard_w, step)

    for shift in range(1, n_tp):
        tok_copy(shift).wait()

    tokens_here = normed[...]
    own_block = pl.ds(pl.multiple_of(sp * block, block), block)
    kv_all[own_block, :] = jnp.dot(
        tokens_here, w_all[:, width : 3 * width], preferred_element_type=F32
    ).astype(BF16)
    logits = jnp.dot(tokens_here, w_all[:, 3 * width :], preferred_element_type=F32)
    lane_row = lax.broadcasted_iota(jnp.int32, (1, LANES), 1)
    offset_row = jnp.zeros((1, LANES), F32)
    for h in range(heads):
        offset_row = jnp.where(lane_row == h, offset_ref[h], offset_row)
    logits = logits + offset_row + jnp.log(jnp.full((1, LANES), n_sp * block, F32))
    log_gates = jnp.minimum(logits, 0.0) - jnp.log1p(jnp.exp(-jnp.abs(logits)))
    row_at = lax.broadcasted_iota(jnp.int32, (block, block), 0)
    col_at = lax.broadcasted_iota(jnp.int32, (block, block), 1)
    seen = col_at <= row_at
    ring_start(1, shard_kv)
    cum_here = jnp.dot(
        jnp.where(seen, 1.0, 0.0).astype(F32), log_gates,
        precision=lax.Precision.HIGHEST, preferred_element_type=F32,
    )
    cum_query[...] = cum_here
    gates[pl.ds(sp, 1)] = cum_here.T[None, :8, :]
    queries = (
        jnp.dot(tokens_here, w_all[:, :width], preferred_element_type=F32).astype(BF16).astype(F32)
        * HEAD_DIM ** (-0.5)
    )
    head_at = lax.broadcasted_iota(jnp.int32, (block, width), 1) // HEAD_DIM
    for h in range(heads):
        q_heads[h] = jnp.where(head_at == h, queries, 0.0).astype(BF16)

    def gate_copy(shift):
        return pltpu.make_async_remote_copy(
            src_ref=gates.at[pl.ds(sp, 1)],
            dst_ref=gates.at[pl.ds(sp, 1)],
            send_sem=gate_send.at[shift - 1],
            recv_sem=gate_recv.at[shift - 1],
            device_id=(lax.rem(sp + shift, n_sp), tp),
            device_id_type=MESH,
        )

    for shift in range(1, n_sp):
        gate_copy(shift).start()
    ring_start(2, shard_wo)

    def scores_of(h, index):
        key_block = kv_all[pl.ds(pl.multiple_of(index * block, block), block), :width]
        scores = lax.dot_general(
            q_heads[h], key_block, CONTRACT_LAST, preferred_element_type=F32
        )
        return scores + cum_query[:, h : h + 1] - gates[index, h : h + 1, :]

    def weighted(h, index, weights):
        value_block = kv_all[pl.ds(pl.multiple_of(index * block, block), block), width:]
        with_ones = jnp.where(head_at == h, value_block.astype(F32), 1.0).astype(BF16)
        return jnp.dot(weights.astype(BF16), with_ones, preferred_element_type=F32)

    for h in range(heads):
        scores = jnp.where(seen, scores_of(h, sp), -1e30)
        top = jnp.max(scores, axis=-1, keepdims=True)
        run_max[h] = top
        run_acc[h] = weighted(h, sp, jnp.where(seen, jnp.exp(scores - top), 0.0))

    def absorb(index):
        for h in range(heads):
            scores = scores_of(h, index)
            old = run_max[h]
            top = jnp.maximum(old, jnp.max(scores, axis=-1, keepdims=True))
            run_max[h] = top
            run_acc[h] = run_acc[h] * jnp.exp(old - top) + weighted(
                h, index, jnp.exp(scores - top)
            )

    for shift in range(1, n_sp):
        gate_copy(shift).wait()

    def shift_back(count, start):
        index = sp - 1 - count
        local_cum = gates[index]
        start = start - local_cum[:, block - 1 :]
        gates[index] = local_cum + start
        return start

    lax.fori_loop(0, sp, shift_back, jnp.zeros((8, 1), F32))

    @pl.loop(1, half + 1)
    def _(step):
        first, second = ring_step(1, shard_kv, step)

        @pl.when(first < sp)
        def _():
            absorb(first)

        @pl.when((step < half) & (second < sp))
        def _():
            absorb(second)

        ring_step(2, shard_wo, step)

    attended = jnp.zeros((block, width), F32)
    for h in range(heads):
        other = ((h + 1) % heads) * HEAD_DIM
        acc = run_acc[h]
        attended = jnp.where(head_at == h, acc / acc[:, other : other + 1], attended)
    partial[...] = lax.dot_general(
        attended.astype(BF16), wo_all[...], CONTRACT_LAST, preferred_element_type=F32
    ).astype(BF16)

    def sum_copy(shift):
        peer = lax.rem(tp + shift, n_tp)
        return pltpu.make_async_remote_copy(
            src_ref=partial.at[pl.ds(pl.multiple_of(peer * rows, rows), rows), :],
            dst_ref=shares.at[shift - 1],
            send_sem=sum_send.at[shift - 1],
            recv_sem=sum_recv.at[shift - 1],
            device_id=(sp, peer),
            device_id_type=MESH,
        )

    for shift in range(1, n_tp):
        sum_copy(shift).start()
    ring_drain(0, shard_w)
    ring_drain(1, shard_kv)
    ring_drain(2, shard_wo)
    total = partial[my_rows, :].astype(F32)
    for shift in range(1, n_tp):
        sum_copy(shift).wait()
        total = total + shares[shift - 1].astype(F32)
    out_ref[...] = rms_norm(total, out_gain_ref[...])


def solution(mesh):
    n_sp, n_tp = mesh.shape["sp"], mesh.shape["tp"]

    def on_device(
        tokens, norm_gain, w_query, w_key, w_value, w_forget, forget_offset, w_out_t, out_gain
    ):
        rows, model = tokens.shape
        w_rows, width = w_query.shape
        heads = w_forget.shape[1]
        block = rows * n_tp
        steps = n_sp // 2 + 1
        vmem = pl.BlockSpec(memory_space=pltpu.VMEM)
        anywhere = pl.BlockSpec(memory_space=pl.ANY)
        dma = pltpu.SemaphoreType.DMA
        return pl.pallas_call(
            functools.partial(layer_kernel, n_sp, n_tp, heads),
            out_shape=jax.ShapeDtypeStruct((rows, model), BF16),
            in_specs=[
                vmem, vmem, anywhere, anywhere, anywhere, vmem,
                pl.BlockSpec(memory_space=pltpu.SMEM), anywhere, vmem,
            ],
            out_specs=vmem,
            scratch_shapes=[
                pltpu.VMEM((block, model), BF16),
                pltpu.VMEM((n_sp * w_rows, 3 * width + LANES), BF16),
                pltpu.VMEM((n_sp * w_rows, width), BF16),
                pltpu.VMEM((n_sp * block, 2 * width), BF16),
                pltpu.VMEM((n_sp, 8, block), F32),
                pltpu.VMEM((heads, block, width), BF16),
                pltpu.VMEM((block, LANES), F32),
                pltpu.VMEM((heads, block, 1), F32),
                pltpu.VMEM((heads, block, width), F32),
                pltpu.VMEM((block, model), BF16),
                pltpu.VMEM((n_tp - 1, rows, model), BF16),
                dma((4,)),
                dma((3, 2, steps)),
                dma((3, 2, steps)),
                dma((n_sp - 1,)),
                dma((n_sp - 1,)),
                dma((n_tp - 1,)),
                dma((n_tp - 1,)),
                dma((n_tp - 1,)),
                dma((n_tp - 1,)),
            ],
            compiler_params=pltpu.CompilerParams(collective_id=0, has_side_effects=True),
        )(
            tokens, norm_gain.reshape(1, model), w_query, w_key, w_value, w_forget,
            forget_offset, w_out_t, out_gain.reshape(1, model),
        )

    return jax.shard_map(
        on_device,
        mesh=mesh,
        in_specs=(
            P(("sp", "tp"), None),
            P(),
            P("sp", "tp"),
            P("sp", "tp"),
            P("sp", "tp"),
            P("sp", "tp"),
            P("tp"),
            P("sp", "tp"),
            P(),
        ),
        out_specs=P(("sp", "tp"), None),
        check_vma=False,
    )
```

time: 257 us -> 72.3 us (0.28)
  blocking collectives: 152 us -> 0 us
  Pallas kernels: 0 us -> 69.1 us
  waiting for transfers between devices: 59.3 us -> 0 us
  matrix products: 16.2 us -> 0 us
  between operations: 13.2 us -> 0.01 us
  other arithmetic: 9.86 us -> 0 us
    all_gather x7 -> x0, blocking collectives: 152 us -> none  [the longest x1 25.8 us: on_device(): lax.all_gather(w_query, 'sp', axis=0, tiled=True)]
    pallas_call x0 -> x1, Pallas kernels: none -> 69.1 us  [on_device(): pl.pallas_call(functools.partial(layer_kernel, n_sp, n_tp, heads), out_sh...]
    all_gather x2 -> x0, waiting for transfers between devices: 36.1 us -> none  [gathered(): return lax.all_gather(part, axis, axis=dim, tiled=True)]
    reduce_scatter x1 -> x0, waiting for transfers between devices: 22.5 us -> none  [own_rows(): lax.psum_scatter(sent, axis, scatter_dimension=0, tiled=True)]
    dot_general x4 -> x0, matrix products: 16.2 us -> none  [the longest x1 10.4 us: absorb(): jnp.einsum('hqk,khd->hqd', shares, value_piece.astype(jnp.float32), preci...]
    reduce_sum x3 -> x0, other arithmetic: 5.3 us -> none  [the longest x1 3.21 us: absorb(): new_sum = run_sum * rescale + jnp.sum(shares, axis=-1)]
    convert_element_type x2 -> x0, other arithmetic: 2.67 us -> none  [rms_norm(): return (floats * scale_row * gain_row).astype(jnp.bfloat16)]
  transfers between devices with their start and end apart: 3 -> 0, of which waited for: 3 -> 0; matrix products, arithmetic and copies ran while one was open for 4% -> 0% of each run, Pallas kernels for 0% -> 0%
where the time goes in v1:
time: 72.3 us; the launch traced here: 72.1 us
  Pallas kernels  69.1 us (96%)
  local copies, waits for them, and re-layouts  2.98 us (4%)
    pallas_call x1, Pallas kernels, on_device(): pl.pallas_call(functools.partial(layer_kernel, n_sp, n_tp, heads), out_sh...  69.1 us
    unnamed x4, local copies, waits for them, and re-layouts  2.98 us

profile of v1, /device:TPU:1, one launch (start us, length us, event | category | flops | bytes accessed | tf_op | source)
XLA Modules:
  0.0 72.1 jit_solution(53528918281672853)
XLA Ops:
  0.0 0.0 copy-start
  0.0 0.7 copy-done
  0.7 0.7 %copy.10.wf_ref = bf16[128,4]{1,0:T(8,128)(2,1)} copy(bf16[128,4]{0,1:T(4,128)(2,1)S(1)} %copy-done) | data formatting | bytes 2048 | tf_op args[5]
  1.4 69.1 %shard_map.91 = bf16[64,1024]{1,0:T(8,128)(2,1)} custom-call(bf16[64,1024]{1,0:T(8,128)(2,1)} %tokens_ref.1, f32[1,1024]{1,0:T(1,128)} %bitcast.2, bf16[128,256]{1,0:T(8,128)(2,1)} %wq_ref.1, bf16[128,256]{1,0:T(8,128)(2,1)} %wk_ref.1, bf16[128,256]{1,0:T(8,128)(2,1)} %wv_ref.1, bf16[128,4]{1,0:T(8,128)(2,1)} %copy.10.wf_ref, f32[4]{0:T(128)} %offset_ref.1, ...), custom_call_target="tpu_custom_call" | custom-call | tf_op jit(solution)/shard_map/pallas_call | solution.py:290
  70.5 1.6 %copy.12 = bf16[64,1024]{1,0:T(8,128)(2,1)} copy(bf16[64,1024]{1,0:T(8,128)(2,1)} %shard_map.91) | data formatting | bytes 262144
Async XLA Ops:
  0.0 0.7 copy-start

commit v2 on v1

--- a/solution.py
+++ b/solution.py
@@ -25,8 +25,8 @@
     n_sp, n_tp, heads,
     tokens_ref, gain_ref, wq_ref, wk_ref, wv_ref, wf_ref, offset_ref, wo_ref, out_gain_ref,
     out_ref,
-    normed, w_all, wo_all, kv_all, gates, q_heads, cum_query, run_max, run_acc, partial, shares,
-    local_sem, send_sem, recv_sem, gate_send, gate_recv, tok_send, tok_recv, sum_send, sum_recv,
+    normed, w_all, wo_all, kv_all, forget_all, gates, q_heads, cum_query, run_max, run_acc, partial, shares,
+    local_sem, send_sem, recv_sem, forget_send, forget_recv, gate_send, gate_recv, tok_send, tok_recv, sum_send, sum_recv,
 ):
     sp, tp = lax.axis_index("sp"), lax.axis_index("tp")
     rows = tokens_ref.shape[0]
@@ -44,53 +44,50 @@
 
     right, left = index_at(place + 1), index_at(place - 1)
 
-    def shard_w(index):
-        return w_all.at[pl.ds(pl.multiple_of(index * w_rows, w_rows), w_rows), :]
-
-    def shard_wo(index):
-        return wo_all.at[pl.ds(pl.multiple_of(index * w_rows, w_rows), w_rows), :]
-
-    def shard_kv(index):
-        return kv_all.at[pl.ds(pl.multiple_of(index * block, block), block), :]
-
-    def hop(ring, shard, way, step, index):
+    def view(ref, index, count, chunk):
+        lanes = ref.shape[1] // 2
+        return ref.at[
+            pl.ds(pl.multiple_of(index * count, count), count), pl.ds(chunk * lanes, lanes)
+        ]
+
+    def hop(ring, chunk, way, step, index):
+        ref, count = ((w_all, w_rows), (kv_all, block), (wo_all, w_rows))[ring]
         return pltpu.make_async_remote_copy(
-            src_ref=shard(index),
-            dst_ref=shard(index),
-            send_sem=send_sem.at[ring, way, step],
-            recv_sem=recv_sem.at[ring, way, step],
+            src_ref=view(ref, index, count, chunk),
+            dst_ref=view(ref, index, count, chunk),
+            send_sem=send_sem.at[ring, chunk, way, step],
+            recv_sem=recv_sem.at[ring, chunk, way, step],
             device_id=((right, left)[way], tp),
             device_id_type=MESH,
         )
 
-    def ring_start(ring, shard):
-        hop(ring, shard, 0, 1, sp).start()
-        if half > 1:
-            hop(ring, shard, 1, 1, sp).start()
-
-    def ring_step(ring, shard, step):
-        first, second = index_at(place - step), index_at(place + step)
-        hop(ring, shard, 0, step, first).wait_recv()
-
-        @pl.when(step < half)
-        def _():
-            hop(ring, shard, 0, step + 1, first).start()
-            hop(ring, shard, 1, step, second).wait_recv()
-
-        @pl.when(step < half - 1)
-        def _():
-            hop(ring, shard, 1, step + 1, second).start()
-
-        return first, second
-
-    def ring_drain(ring, shard):
-        @pl.loop(1, half + 1)
-        def _(step):
-            hop(ring, shard, 0, step, sp).wait_send()
-
-            @pl.when(step < half)
+    lanes_of_ring = [(c, w, half if c == w else half - 1) for c in (0, 1) for w in (c, 1 - c)]
+
+    def ring_start(ring):
+        for chunk, way, last in lanes_of_ring:
+            if last > 0:
+                hop(ring, chunk, way, 1, sp).start()
+
+    def ring_step(ring, step):
+        arrived = index_at(place - step), index_at(place + step)
+        for chunk, way, last in lanes_of_ring:
+
+            @pl.when(step <= last)
             def _():
-                hop(ring, shard, 1, step, sp).wait_send()
+                hop(ring, chunk, way, step, arrived[way]).wait_recv()
+
+                @pl.when(step < last)
+                def _():
+                    hop(ring, chunk, way, step + 1, arrived[way]).start()
+
+        return arrived
+
+    def ring_drain(ring):
+        for chunk, way, last in lanes_of_ring:
+
+            @pl.loop(1, last + 1)
+            def _(step):
+                hop(ring, chunk, way, step, sp).wait_send()
 
     own_rows = pl.ds(pl.multiple_of(sp * w_rows, w_rows), w_rows)
     local = [
@@ -111,17 +108,31 @@
             barrier, inc=1, device_id=(sp, lax.rem(tp + shift, n_tp)), device_id_type=MESH
         )
 
-    forget = jnp.concatenate(
-        [wf_ref[...].astype(F32), jnp.zeros((w_rows, LANES - heads), F32)], axis=1
-    )
-    w_all[own_rows, 3 * width :] = forget.astype(BF16)
+    forget_all[pl.ds(sp, 1)] = jnp.concatenate(
+        [wf_ref[...].astype(F32), jnp.zeros((8 - heads, w_rows), F32)], axis=0
+    )[None]
     my_rows = pl.ds(pl.multiple_of(tp * rows, rows), rows)
     normed[my_rows, :] = rms_norm(tokens_ref[...].astype(F32), gain_ref[...])
     for copy in local:
         copy.wait()
     pl.semaphore_wait(barrier, n_sp + n_tp - 2)
 
-    ring_start(0, shard_w)
+    def spread(ref, sends, receives):
+        return [
+            pltpu.make_async_remote_copy(
+                src_ref=ref.at[pl.ds(sp, 1)],
+                dst_ref=ref.at[pl.ds(sp, 1)],
+                send_sem=sends.at[shift - 1],
+                recv_sem=receives.at[shift - 1],
+                device_id=(lax.rem(sp + shift, n_sp), tp),
+                device_id_type=MESH,
+            )
+            for shift in range(1, n_sp)
+        ]
+
+    forget_copies = spread(forget_all, forget_send, forget_recv)
+    for copy in forget_copies:
+        copy.start()
 
     def tok_copy(shift):
         return pltpu.make_async_remote_copy(
@@ -135,36 +146,48 @@
 
     for shift in range(1, n_tp):
         tok_copy(shift).start()
-
-    @pl.loop(1, half + 1)
+    ring_start(0)
+
+    @pl.loop(1, half)
     def _(step):
-        ring_step(0, shard_w, step)
+        ring_step(0, step)
 
     for shift in range(1, n_tp):
         tok_copy(shift).wait()
+    for copy in forget_copies:
+        copy.wait()
 
     tokens_here = normed[...]
-    own_block = pl.ds(pl.multiple_of(sp * block, block), block)
-    kv_all[own_block, :] = jnp.dot(
-        tokens_here, w_all[:, width : 3 * width], preferred_element_type=F32
-    ).astype(BF16)
-    logits = jnp.dot(tokens_here, w_all[:, 3 * width :], preferred_element_type=F32)
-    lane_row = lax.broadcasted_iota(jnp.int32, (1, LANES), 1)
-    offset_row = jnp.zeros((1, LANES), F32)
+    forget_rows = jnp.concatenate([forget_all[i] for i in range(n_sp)], axis=1).astype(BF16)
+    logits = lax.dot_general(
+        forget_rows, tokens_here, CONTRACT_LAST, preferred_element_type=F32
+    )
+    head_row = lax.broadcasted_iota(jnp.int32, (8, block), 0)
+    offsets = jnp.zeros((8, block), F32)
     for h in range(heads):
-        offset_row = jnp.where(lane_row == h, offset_ref[h], offset_row)
-    logits = logits + offset_row + jnp.log(jnp.full((1, LANES), n_sp * block, F32))
+        offsets = jnp.where(head_row == h, offset_ref[h], offsets)
+    logits = logits + offsets + jnp.log(jnp.full((8, block), n_sp * block, F32))
     log_gates = jnp.minimum(logits, 0.0) - jnp.log1p(jnp.exp(-jnp.abs(logits)))
     row_at = lax.broadcasted_iota(jnp.int32, (block, block), 0)
     col_at = lax.broadcasted_iota(jnp.int32, (block, block), 1)
     seen = col_at <= row_at
-    ring_start(1, shard_kv)
     cum_here = jnp.dot(
-        jnp.where(seen, 1.0, 0.0).astype(F32), log_gates,
+        log_gates, jnp.where(row_at <= col_at, 1.0, 0.0).astype(F32),
         precision=lax.Precision.HIGHEST, preferred_element_type=F32,
     )
-    cum_query[...] = cum_here
-    gates[pl.ds(sp, 1)] = cum_here.T[None, :8, :]
+    gates[pl.ds(sp, 1)] = cum_here[None]
+    cum_query[...] = jnp.concatenate([cum_here, jnp.zeros((LANES - 8, block), F32)], axis=0).T
+    gate_copies = spread(gates, gate_send, gate_recv)
+    for copy in gate_copies:
+        copy.start()
+    ring_step(0, half)
+
+    ring_start(2)
+    own_block = pl.ds(pl.multiple_of(sp * block, block), block)
+    kv_all[own_block, :] = jnp.dot(
+        tokens_here, w_all[:, width:], preferred_element_type=F32
+    ).astype(BF16)
+    ring_start(1)
     queries = (
         jnp.dot(tokens_here, w_all[:, :width], preferred_element_type=F32).astype(BF16).astype(F32)
         * HEAD_DIM ** (-0.5)
@@ -172,20 +195,6 @@
     head_at = lax.broadcasted_iota(jnp.int32, (block, width), 1) // HEAD_DIM
     for h in range(heads):
         q_heads[h] = jnp.where(head_at == h, queries, 0.0).astype(BF16)
-
-    def gate_copy(shift):
-        return pltpu.make_async_remote_copy(
-            src_ref=gates.at[pl.ds(sp, 1)],
-            dst_ref=gates.at[pl.ds(sp, 1)],
-            send_sem=gate_send.at[shift - 1],
-            recv_sem=gate_recv.at[shift - 1],
-            device_id=(lax.rem(sp + shift, n_sp), tp),
-            device_id_type=MESH,
-        )
-
-    for shift in range(1, n_sp):
-        gate_copy(shift).start()
-    ring_start(2, shard_wo)
 
     def scores_of(h, index):
         key_block = kv_all[pl.ds(pl.multiple_of(index * block, block), block), :width]
@@ -215,8 +224,8 @@
                 h, index, jnp.exp(scores - top)
             )
 
-    for shift in range(1, n_sp):
-        gate_copy(shift).wait()
+    for copy in gate_copies:
+        copy.wait()
 
     def shift_back(count, start):
         index = sp - 1 - count
@@ -226,10 +235,11 @@
         return start
 
     lax.fori_loop(0, sp, shift_back, jnp.zeros((8, 1), F32))
+    ring_step(2, 1)
 
     @pl.loop(1, half + 1)
     def _(step):
-        first, second = ring_step(1, shard_kv, step)
+        first, second = ring_step(1, step)
 
         @pl.when(first < sp)
         def _():
@@ -239,7 +249,9 @@
         def _():
             absorb(second)
 
-        ring_step(2, shard_wo, step)
+        @pl.when(step < half)
+        def _():
+            ring_step(2, step + 1)
 
     attended = jnp.zeros((block, width), F32)
     for h in range(heads):
@@ -263,9 +275,8 @@
 
     for shift in range(1, n_tp):
         sum_copy(shift).start()
-    ring_drain(0, shard_w)
-    ring_drain(1, shard_kv)
-    ring_drain(2, shard_wo)
+    for ring in range(3):
+        ring_drain(ring)
     total = partial[my_rows, :].astype(F32)
     for shift in range(1, n_tp):
         sum_copy(shift).wait()
@@ -297,9 +308,10 @@
             out_specs=vmem,
             scratch_shapes=[
                 pltpu.VMEM((block, model), BF16),
-                pltpu.VMEM((n_sp * w_rows, 3 * width + LANES), BF16),
+                pltpu.VMEM((n_sp * w_rows, 3 * width), BF16),
                 pltpu.VMEM((n_sp * w_rows, width), BF16),
                 pltpu.VMEM((n_sp * block, 2 * width), BF16),
+                pltpu.VMEM((n_sp, 8, w_rows), F32),
                 pltpu.VMEM((n_sp, 8, block), F32),
                 pltpu.VMEM((heads, block, width), BF16),
                 pltpu.VMEM((block, LANES), F32),
@@ -308,8 +320,10 @@
                 pltpu.VMEM((block, model), BF16),
                 pltpu.VMEM((n_tp - 1, rows, model), BF16),
                 dma((4,)),
-                dma((3, 2, steps)),
-                dma((3, 2, steps)),
+                dma((3, 2, 2, steps)),
+                dma((3, 2, 2, steps)),
+                dma((n_sp - 1,)),
+                dma((n_sp - 1,)),
                 dma((n_sp - 1,)),
                 dma((n_sp - 1,)),
                 dma((n_tp - 1,)),
@@ -319,7 +333,7 @@
             ],
             compiler_params=pltpu.CompilerParams(collective_id=0, has_side_effects=True),
         )(
-            tokens, norm_gain.reshape(1, model), w_query, w_key, w_value, w_forget,
+            tokens, norm_gain.reshape(1, model), w_query, w_key, w_value, w_forget.T,
             forget_offset, w_out_t, out_gain.reshape(1, model),
         )
 

time: 72.3 us -> 62 us (0.86)
  Pallas kernels: 69.1 us -> 60.2 us
  local copies, waits for them, and re-layouts: 2.98 us -> 1.57 us
    pallas_call x1, Pallas kernels: 69.1 us -> 60.2 us  [on_device(): pl.pallas_call(functools.partial(layer_kernel, n_sp, n_tp, heads), out_sh...]
    unnamed x4 -> x1, local copies, waits for them, and re-layouts: 2.98 us -> 1.57 us
where the time goes in v2:
time: 62 us; the launch traced here: 61.8 us
  Pallas kernels  60.2 us (97%)
  local copies, waits for them, and re-layouts  1.57 us (3%)
    pallas_call x1, Pallas kernels, on_device(): pl.pallas_call(functools.partial(layer_kernel, n_sp, n_tp, heads), out_sh...  60.2 us
    unnamed x1, local copies, waits for them, and re-layouts  1.57 us

profile of v2, /device:TPU:1, one launch (start us, length us, event | category | flops | bytes accessed | tf_op | source)
XLA Modules:
  0.0 61.8 jit_solution(18163082682882462450)
XLA Ops:
  0.0 60.2 %shard_map.91 = bf16[64,1024]{1,0:T(8,128)(2,1)} custom-call(bf16[64,1024]{1,0:T(8,128)(2,1)} %tokens_ref.1, f32[1,1024]{1,0:T(1,128)} %bitcast.3, bf16[128,256]{1,0:T(8,128)(2,1)} %wq_ref.1, bf16[128,256]{1,0:T(8,128)(2,1)} %wk_ref.1, bf16[128,256]{1,0:T(8,128)(2,1)} %wv_ref.1, bf16[4,128]{1,0:T(4,128)(2,1)} %bitcast.5, f32[4]{0:T(128)} %offset_ref.1, ...), custom_call_target="tpu_custom_call" | custom-call | tf_op jit(solution)/shard_map/pallas_call | solution.py:301
  60.2 1.6 %copy.11 = bf16[64,1024]{1,0:T(8,128)(2,1)} copy(bf16[64,1024]{1,0:T(8,128)(2,1)} %shard_map.91) | data formatting | bytes 262144
